TPU v7x, 512 devices: a whole 4x8x8 slice. The times are simulated.
512 devices in a mesh: fs: 64 (over z, y), tp: 8 (over x, core).
Axes of the slice: x: 4, y: 8, z: 8, core: 2. Of those that a mesh axis runs over, the one named last changes fastest.
Arguments:
- saved_inputs: bfloat16 [49152, 2048], P('fs'), may hold values from -16 to 16
- cotangents: bfloat16 [3, 49152, 1024], P(None, 'fs', 'tp'), may hold values from -0.02734375 to 0.02734375
- left_roots: float32 [3, 2048, 2048], P(None, 'fs'), may hold values from -1 to 2
- right_roots: float32 [3, 1024, 128], P(None, 'tp'), may hold values from -1 to 2
- moments: float32 [3, 2048, 1024], P(None, 'fs', 'tp'), may hold values from -125 to 125
- masters: float32 [3, 2048, 1024], P(None, 'fs', 'tp'), may hold values from -3 to 3
Outputs:
- direction: float32 [3, 2048, 1024], P(None, 'fs', 'tp')
- moments_new: float32 [3, 2048, 1024], P(None, 'fs', 'tp')
- copies: bfloat16 [3, 2048, 1024], P(None, None, 'tp')
All inputs are finite; a program needn't handle non-finite values.
Results may differ from a plain program's by a relative error of at most 0.002.
Values may be sent and summed in bfloat16 or wider, within the bound.
A program may use at most 64 MiB of HBM per device.

v0:
```python
import jax
import jax.numpy as jnp
from jax import lax
from jax.sharding import Mesh
from jax.sharding import PartitionSpec as P

D = 2048
SBW = 1024
RB = 128
FS = ("fs_0", "fs_1")
TP = ("tp_0", "tp_1")
momentum_decay = 0.9
step_rate = 0.1
eps_value = 1e-06


def filled_up(lines, peers):
    spare = -len(lines) % peers
    return jnp.pad(lines, [(0, spare)] + [(0, 0)] * (lines.ndim - 1))


def in_order(pieces, dim):
    lengths = list(pieces.shape[1:])
    lengths[dim] *= pieces.shape[0]
    return jnp.moveaxis(pieces, 0, dim).reshape(lengths)


def from_everyone(value, axis):
    peers = lax.axis_size(axis)
    return lax.all_to_all(
        jnp.broadcast_to(value[None], (peers, *value.shape)), axis, 0, 0, tiled=True
    )


def collect(value, axis, dim):
    return in_order(from_everyone(value, axis), dim)


def in_blocks(value, dim, peers):
    before, after = (value.shape[:dim], value.shape[dim + 1 :])
    return jnp.moveaxis(value.reshape(*before, peers, -1, *after), dim, 0)


def summed_on_arrival(value, axis, dim):
    peers = lax.axis_size(axis)
    pieces = lax.all_to_all(in_blocks(value, dim, peers), axis, 0, 0, tiled=True)
    return jnp.sum(pieces.astype(jnp.float32), axis=0)


def nested_sum(value, axes):
    lines = value.reshape(-1, value.shape[-1])
    padded = filled_up(lines, lax.axis_size(axes))
    whole = collect(summed_on_arrival(padded, axes, 0).astype(jnp.bfloat16), axes, 0)
    return lax.slice_in_dim(whole, 0, len(lines)).reshape(value.shape).astype(jnp.float32)


def taken_together(value, axis):
    everything = from_everyone(value, axis)
    return jnp.sum(everything, axis=0)


def by_axis(value, axes):
    far, near = axes
    nearer = taken_together(value, near)
    return taken_together(nearer, far)


def on_device(saved_inputs, cotangents, left_roots, right_roots, moments, masters):
    rows_own = masters.shape[1]
    columns = masters.shape[2]
    partial_value = jnp.einsum(
        "td,mtc->dmc", saved_inputs, cotangents, preferred_element_type=jnp.float32
    )
    summed = nested_sum(partial_value.astype(jnp.bfloat16), FS)
    left_done = jnp.einsum("mrd,dmc->mrc", left_roots, summed, precision=lax.Precision.HIGHEST)
    block_count = columns // RB
    right_blocks = right_roots.reshape(3, block_count, RB, RB)
    right_done = jnp.einsum(
        "mrbi,mbij->mrbj",
        left_done.reshape(3, rows_own, block_count, RB),
        right_blocks,
        precision=lax.Precision.HIGHEST,
    ).reshape(3, rows_own, columns)
    moments_new = momentum_decay * moments + right_done
    totals = by_axis(
        jnp.sum(moments_new * moments_new, axis=(1, 2)), (("fs_0", "fs_1"), ("tp_0", "tp_1"))
    )
    meansq = totals / (D * SBW)
    direction = moments_new * lax.rsqrt(meansq + eps_value)[:, None, None]
    copy_rows = (masters - step_rate * direction).astype(jnp.bfloat16)
    copies = lax.all_gather(copy_rows, FS, axis=1, tiled=True)
    return (direction, moments_new, copies)


def solution(mesh):
    torus = Mesh(mesh.devices.reshape(8, 8, 4, 2), ("fs_0", "fs_1", "tp_0", "tp_1"))
    in_specs = (
        P(FS, None),
        P(None, FS, TP),
        P(None, FS, None),
        P(None, TP, None),
        P(None, FS, TP),
        P(None, FS, TP),
    )
    out_specs = (P(None, FS, TP), P(None, FS, TP), P(None, None, TP))
    return jax.shard_map(
        on_device, mesh=torus, in_specs=in_specs, out_specs=out_specs, check_vma=False
    )
```

profile of v0, /device:TPU:2, one launch (start us, length us, event | category | flops | bytes accessed | tf_op | source)
XLA Modules:
  0.0 252.0 jit_solution(6863095140001499343)
XLA Ops:
  7.2 0.0 copy-start
  7.2 0.0 all-gather.2.cloned.1.call-start
  7.2 1.8 copy-done
  9.1 2.9 %fusion.2 = bf16[2048,3,128]{2,0,1:T(8,128)(2,1)S(1)} fusion(bf16[3,768,128]{2,1,0:T(8,128)(2,1)} %param.7, bf16[768,2048]{1,0:T(8,128)(2,1)S(1)} %copy-done), kind=kOutput, calls=%fused_computation.2 | convolution fusion | flops 1208745984 | bytes 5308416 | tf_op jit(solution)/shard_map/td,mtc->dmc/dot_general | solution.py:71
  12.0 10.8 %copy.21 = bf16[2048,3,128]{2,1,0:T(4,128)(2,1)} copy(bf16[2048,3,128]{2,0,1:T(8,128)(2,1)S(1)} %fusion.2) | data formatting | bytes 3145728 | tf_op jit(solution)/shard_map/convert_element_type | solution.py:74
  22.7 5.0 %reshape.37 = bf16[64,96,128]{2,1,0:T(8,128)(2,1)} reshape(bf16[2048,3,128]{2,1,0:T(4,128)(2,1)} %copy.21) | data formatting | bytes 3145728 | tf_op jit(solution)/shard_map/reshape | solution.py:41
  27.8 58.0 %all_to_all.22 = bf16[64,96,128]{2,1,0:T(8,128)(2,1)} all-to-all(bf16[64,96,128]{2,1,0:T(8,128)(2,1)} %reshape.37), channel_id=1, replica_groups=mesh['fs_0'=8,'fs_1'=8,'tp_0'=4,'tp_1'=2] {'fs_0','fs_1'}, dimensions={0} | all-to-all | bytes 3145728 | tf_op jit(solution)/shard_map/all_to_all | solution.py:46
  85.8 1.7 reduce_sum.39
  87.4 0.2 broadcast_in_dim.6
  87.6 47.3 %all_to_all.23 = bf16[64,96,128]{2,1,0:T(8,128)(2,1)} all-to-all(bf16[64,96,128]{2,1,0:T(8,128)(2,1)S(1)} %broadcast_in_dim.6), channel_id=1, replica_groups=mesh['fs_0'=8,'fs_1'=8,'tp_0'=4,'tp_1'=2] {'fs_0','fs_1'}, dimensions={0} | all-to-all | bytes 3145728 | tf_op jit(solution)/shard_map/all_to_all | solution.py:30
  134.9 5.2 %reshape_reshape.3 = bf16[2048,3,128]{2,1,0:T(4,128)(2,1)} reshape(bf16[64,96,128]{2,1,0:T(8,128)(2,1)} %all_to_all.23) | data formatting | bytes 3145728 | tf_op jit(solution)/shard_map/reshape;reshape | solution.py:54
  140.1 2.6 %fusion.5 = f32[3,128,32]{1,2,0:T(8,128)S(1)} fusion(f32[3,32,2048]{2,1,0:T(8,128)} %param.8, bf16[2048,3,128]{2,1,0:T(4,128)(2,1)} %reshape_reshape.3), kind=kOutput, calls=%fused_computation.3 | convolution fusion | flops 301989888 | bytes 2408448 | tf_op jit(solution)/shard_map/mrd,dmc->mrc/dot_general | solution.py:75
  142.7 0.0 copy-done.1
  142.7 0.0 copy-done.4
  142.8 0.4 multiply_reduce_fusion
  143.1 8.5 %all_to_all.24 = f32[8,1,3]{2,1,0:T(1,128)S(1)} all-to-all(f32[8,1,3]{2,1,0:T(1,128)S(1)} %broadcast_in_dim.7), channel_id=1, replica_groups=mesh['fs_0'=8,'fs_1'=8,'tp_0'=4,'tp_1'=2] {'tp_0','tp_1'}, dimensions={0} | all-to-all | bytes 192 | tf_op jit(solution)/shard_map/all_to_all | solution.py:30
  151.7 18.5 %all_to_all.25 = f32[64,1,3]{2,1,0:T(1,128)S(1)} all-to-all(f32[64,1,3]{2,1,0:T(1,128)S(1)} %broadcast_in_dim.8), channel_id=1, replica_groups=mesh['fs_0'=8,'fs_1'=8,'tp_0'=4,'tp_1'=2] {'fs_0','fs_1'}, dimensions={0} | all-to-all | bytes 1536 | tf_op jit(solution)/shard_map/all_to_all | solution.py:30
  170.2 0.1 reduce_sum.42
  170.3 0.0 copy-done.3
  170.3 0.7 subtract_convert_fusion
  171.0 0.0 all-gather.2.cloned.1.call-update
  171.0 71.5 %all-gather.2.cloned.1.call-done = bf16[3,2048,128]{2,1,0:T(8,128)(2,1)} async-done(((bf16[3,32,128]{2,1,0:T(8,128)(2,1)}), bf16[3,2048,128]{2,1,0:T(8,128)(2,1)}) %all-gather.2.cloned.1.call-update) | async-done | bytes 1572880 | tf_op jit(solution)/shard_map/all_gather | solution.py:91
  242.5 2.7 %copy.32 = bf16[3,2048,128]{2,1,0:T(8,128)(2,1)} copy(bf16[3,2048,128]{2,1,0:T(8,128)(2,1)} %all-gather.2.cloned.1.call-done) | data formatting | bytes 3145728
  245.2 0.0 copy-done.2
  (8 shorter events, 0.1 us)
Async XLA Ops:
  7.2 1.9 copy-start
  7.2 235.3 %all-gather.2.cloned.1.call-start = ((), (), s32[]{:S(2)}) async-start(), calls=%async_computation.4 | async-start | bytes 1597440 | tf_op jit(solution)/shard_map/all_gather | solution.py:91
  140.1 2.6 %copy-start.1 = (f32[3,128,128]{2,1,0:T(8,128)S(1)}, f32[3,128,128]{2,1,0:T(8,128)}, u32[]{:S(2)}) copy-start(f32[3,128,128]{2,1,0:T(8,128)} %param.9) | copy-start | bytes 589828
  140.1 2.7 %copy-start.4 = (f32[3,32,128]{2,1,0:T(8,128)S(1)}, f32[3,32,128]{2,1,0:T(8,128)}, u32[]{:S(2)}) copy-start(f32[3,32,128]{2,1,0:T(8,128)} %param.10) | copy-start | bytes 147460
  140.1 30.2 %copy-start.3 = (f32[3,32,128]{2,1,0:T(8,128)S(1)}, f32[3,32,128]{2,1,0:T(8,128)}, u32[]{:S(2)}) copy-start(f32[3,32,128]{2,1,0:T(8,128)} %param.11) | copy-start | bytes 147460
  143.1 102.0 %copy-start.2 = (f32[3,32,128]{2,1,0:T(8,128)}, f32[3,32,128]{2,1,0:T(8,128)S(1)}, u32[]{:S(2)}) copy-start(f32[3,32,128]{2,1,0:T(8,128)S(1)} %get-tuple-element.11) | copy-start | bytes 147460
Sparse Core Ops, SparseCore 0:
  171.1 71.3 all-gather.1
where the time goes:
time: 253 us; the launch traced here: 252 us
  blocking collectives  132 us (52%)
  waiting for transfers between devices  71.5 us (28%)
  local copies, waits for them, and re-layouts  25.7 us (10%)
  between operations  14.1 us (6%)
  matrix products  5.9 us (2%)
    all_to_all x3, blocking collectives, from_everyone(): lax.all_to_all(jnp.broadcast_to(value[None], (peers, *value.shape)), axis...  74.3 us
    all_gather x1, waiting for transfers between devices, on_device(): copies = lax.all_gather(copy_rows, FS, axis=1, tiled=True)  71.5 us
    all_to_all x1, blocking collectives, summed_on_arrival(): lax.all_to_all(in_blocks(value, dim, peers), axis, 0, 0, tiled=True)  58 us
    convert_element_type x1, local copies, waits for them, and re-layouts, on_device(): summed = nested_sum(partial_value.astype(jnp.bfloat16), FS)  10.8 us
    another operation x1, local copies, waits for them, and re-layouts, nested_sum(): lax.slice_in_dim(whole, 0, len(lines)).reshape(value.shape)  5.19 us
  transfers between devices with their start and end apart: 1, of which 1 were waited for; matrix products, arithmetic and copies ran while one was open for 0% of the time, Pallas kernels for 0%

commit v1 on v0

--- a/solution.py
+++ b/solution.py
@@ -88,7 +88,9 @@
     meansq = totals / (D * SBW)
     direction = moments_new * lax.rsqrt(meansq + eps_value)[:, None, None]
     copy_rows = (masters - step_rate * direction).astype(jnp.bfloat16)
-    copies = lax.all_gather(copy_rows, FS, axis=1, tiled=True)
+    copies = jnp.concatenate(
+        lax.all_to_all(jnp.stack([copy_rows] * lax.axis_size(FS)), FS, 0, 0), axis=1
+    )
     return (direction, moments_new, copies)
 
 

time: 253 us -> 211 us (0.83)
  the two profiles are of different devices: /device:TPU:2 before, /device:TPU:8 now
where the time goes in v1:
time: 211 us; the launch traced here: 210 us
  blocking collectives  176 us (83%)
  local copies, waits for them, and re-layouts  24.7 us (12%)
  matrix products  5.91 us (3%)
  other arithmetic  2.47 us (1%)
    all_to_all x3, blocking collectives, from_everyone(): lax.all_to_all(jnp.broadcast_to(value[None], (peers, *value.shape)), axis...  74.6 us
    all_to_all x1, blocking collectives, summed_on_arrival(): lax.all_to_all(in_blocks(value, dim, peers), axis, 0, 0, tiled=True)  57.5 us
    all_to_all x1, blocking collectives, on_device(): lax.all_to_all(jnp.stack([copy_rows] * lax.axis_size(FS)), FS, 0, 0)  44.3 us
    convert_element_type x1, local copies, waits for them, and re-layouts, on_device(): summed = nested_sum(partial_value.astype(jnp.bfloat16), FS)  10.8 us
    another operation x1, local copies, waits for them, and re-layouts, nested_sum(): lax.slice_in_dim(whole, 0, len(lines)).reshape(value.shape)  5.19 us
    reshape x1, local copies, waits for them, and re-layouts, in_blocks(): return jnp.moveaxis(value.reshape(*before, peers, -1, *after), dim, 0)  5.01 us

profile of v1, /device:TPU:8, one launch (start us, length us, event | category | flops | bytes accessed | tf_op | source)
XLA Modules:
  0.0 210.3 jit_solution(839805300357958177)
XLA Ops:
  0.6 0.0 copy-start
  0.6 1.9 copy-done
  2.5 2.9 %fusion.2 = bf16[2048,3,128]{2,0,1:T(8,128)(2,1)S(1)} fusion(bf16[3,768,128]{2,1,0:T(8,128)(2,1)} %param.7, bf16[768,2048]{1,0:T(8,128)(2,1)S(1)} %copy-done), kind=kOutput, calls=%fused_computation.2 | convolution fusion | flops 1208745984 | bytes 5308416 | tf_op jit(solution)/shard_map/td,mtc->dmc/dot_general | solution.py:71
  5.4 10.8 %copy.30 = bf16[2048,3,128]{2,1,0:T(4,128)(2,1)} copy(bf16[2048,3,128]{2,0,1:T(8,128)(2,1)S(1)} %fusion.2) | data formatting | bytes 3145728 | tf_op jit(solution)/shard_map/convert_element_type | solution.py:74
  16.2 5.0 %reshape.45 = bf16[64,96,128]{2,1,0:T(8,128)(2,1)} reshape(bf16[2048,3,128]{2,1,0:T(4,128)(2,1)} %copy.30) | data formatting | bytes 3145728 | tf_op jit(solution)/shard_map/reshape | solution.py:41
  21.2 57.5 %all_to_all.27 = bf16[64,96,128]{2,1,0:T(8,128)(2,1)} all-to-all(bf16[64,96,128]{2,1,0:T(8,128)(2,1)} %reshape.45), channel_id=1, replica_groups=mesh['fs_0'=8,'fs_1'=8,'tp_0'=4,'tp_1'=2] {'fs_0','fs_1'}, dimensions={0} | all-to-all | bytes 3145728 | tf_op jit(solution)/shard_map/all_to_all | solution.py:46
  78.8 1.7 reduce_sum.39
  80.4 0.2 broadcast_in_dim.6
  80.6 47.3 %all_to_all.28 = bf16[64,96,128]{2,1,0:T(8,128)(2,1)} all-to-all(bf16[64,96,128]{2,1,0:T(8,128)(2,1)S(1)} %broadcast_in_dim.6), channel_id=1, replica_groups=mesh['fs_0'=8,'fs_1'=8,'tp_0'=4,'tp_1'=2] {'fs_0','fs_1'}, dimensions={0} | all-to-all | bytes 3145728 | tf_op jit(solution)/shard_map/all_to_all | solution.py:30
  127.9 5.2 %reshape_reshape.3 = bf16[2048,3,128]{2,1,0:T(4,128)(2,1)} reshape(bf16[64,96,128]{2,1,0:T(8,128)(2,1)} %all_to_all.28) | data formatting | bytes 3145728 | tf_op jit(solution)/shard_map/reshape;reshape | solution.py:54
  133.1 0.0 copy-start.1
  133.1 2.6 %fusion.5 = f32[3,128,32]{1,2,0:T(8,128)S(1)} fusion(f32[3,32,2048]{2,1,0:T(8,128)} %param.8, bf16[2048,3,128]{2,1,0:T(4,128)(2,1)} %reshape_reshape.3), kind=kOutput, calls=%fused_computation.3 | convolution fusion | flops 301989888 | bytes 2408448 | tf_op jit(solution)/shard_map/mrd,dmc->mrc/dot_general | solution.py:75
  135.8 0.0 copy-done.1
  135.8 0.0 copy-done.4
  135.8 0.4 multiply_reduce_fusion
  136.2 9.4 %all_to_all.29 = f32[8,1,3]{2,1,0:T(1,128)S(1)} all-to-all(f32[8,1,3]{2,1,0:T(1,128)S(1)} %broadcast_in_dim.7), channel_id=1, replica_groups=mesh['fs_0'=8,'fs_1'=8,'tp_0'=4,'tp_1'=2] {'tp_0','tp_1'}, dimensions={0} | all-to-all | bytes 192 | tf_op jit(solution)/shard_map/all_to_all | solution.py:30
  145.6 17.9 %all_to_all.30 = f32[64,1,3]{2,1,0:T(1,128)S(1)} all-to-all(f32[64,1,3]{2,1,0:T(1,128)S(1)} %broadcast_in_dim.8), channel_id=1, replica_groups=mesh['fs_0'=8,'fs_1'=8,'tp_0'=4,'tp_1'=2] {'fs_0','fs_1'}, dimensions={0} | all-to-all | bytes 1536 | tf_op jit(solution)/shard_map/all_to_all | solution.py:30
  163.5 0.1 reduce_sum.42
  163.6 0.0 copy-done.3
  163.6 0.7 subtract_convert_fusion
  164.3 0.2 stack.2
  164.5 44.3 %all_to_all.31 = bf16[64,3,32,128]{3,2,1,0:T(8,128)(2,1)S(1)} all-to-all(bf16[64,3,32,128]{3,2,1,0:T(8,128)(2,1)S(1)} %stack.2), channel_id=1, replica_groups=mesh['fs_0'=8,'fs_1'=8,'tp_0'=4,'tp_1'=2] {'fs_0','fs_1'}, dimensions={0} | all-to-all | bytes 3145728 | tf_op jit(solution)/shard_map/all_to_all | solution.py:92
  208.9 0.0 copy-done.2
  208.9 1.4 copy.34
  (7 shorter events, 0.1 us)
Async XLA Ops:
  0.6 1.9 copy-start
  133.1 2.6 %copy-start.1 = (f32[3,128,128]{2,1,0:T(8,128)S(1)}, f32[3,128,128]{2,1,0:T(8,128)}, u32[]{:S(2)}) copy-start(f32[3,128,128]{2,1,0:T(8,128)} %param.9) | copy-start | bytes 589828
  133.1 2.7 %copy-start.4 = (f32[3,32,128]{2,1,0:T(8,128)S(1)}, f32[3,32,128]{2,1,0:T(8,128)}, u32[]{:S(2)}) copy-start(f32[3,32,128]{2,1,0:T(8,128)} %param.10) | copy-start | bytes 147460
  133.1 30.5 %copy-start.3 = (f32[3,32,128]{2,1,0:T(8,128)S(1)}, f32[3,32,128]{2,1,0:T(8,128)}, u32[]{:S(2)}) copy-start(f32[3,32,128]{2,1,0:T(8,128)} %param.11) | copy-start | bytes 147460
  136.1 72.7 %copy-start.2 = (f32[3,32,128]{2,1,0:T(8,128)}, f32[3,32,128]{2,1,0:T(8,128)S(1)}, u32[]{:S(2)}) copy-start(f32[3,32,128]{2,1,0:T(8,128)S(1)} %get-tuple-element.6) | copy-start | bytes 147460
